TPU v7x, 32 devices: a whole 2x2x4 slice. The times are simulated.
32 devices in a mesh: grp: 2 (over y), ra: 4 (over z), cb: 4 (over x, core).
Axes of the slice: x: 2, y: 2, z: 4, core: 2. Of those that a mesh axis runs over, the one named last changes fastest.
Arguments:
- residual: bfloat16 [512, 4096], P('grp', 'ra'), parts along dimension 0, may hold values from -6 to 6
- gain_first: bfloat16 [4096], P('ra'), may hold values from 0.099609375 to 1.8984375
- gate_first: bfloat16 [4096, 11264], P('ra', 'cb'), may hold values from -0.09375 to 0.09375
- up_first: bfloat16 [4096, 11264], P('ra', 'cb'), may hold values from -0.09375 to 0.09375
- down_first: bfloat16 [11264, 4096], P('cb', 'ra'), may hold values from -0.078125 to 0.078125
- gain_second: bfloat16 [4096], P('ra'), may hold values from 0.099609375 to 1.8984375
- gate_second: bfloat16 [4096, 11264], P('ra', 'cb'), may hold values from -0.09375 to 0.09375
- up_second: bfloat16 [4096, 11264], P('ra', 'cb'), may hold values from -0.09375 to 0.09375
- down_second: bfloat16 [11264, 4096], P('cb', 'ra'), may hold values from -0.078125 to 0.078125
Outputs:
- updated: bfloat16 [512, 4096], P('grp', 'ra'), parts along dimension 0
There are 2 independent parts, one for each index of `grp`. A program takes and returns all parts, laid end to end along the dimension named above; an argument that names none is the same for every part. Nothing has to cross between parts.
All inputs are finite; a program needn't handle non-finite values.
Results may differ from a plain program's by a relative error of at most 0.0071.
Values may be sent and summed in bfloat16 or wider, within the bound.
A program may use at most 128 MiB of HBM per device.

v0:
```python
import functools

import jax
import jax.numpy as jnp
from jax import lax
from jax.experimental import pallas as pl
from jax.experimental.pallas import tpu as pltpu
from jax.sharding import PartitionSpec as P

MESH = pl.DeviceIdType.MESH
LANES = 128
epsilon = 1e-06

HOP = 4
REDUCE = 4
SPREAD = 4
TILE = 8


def kernel(
    cfg,
    residual,
    gain_first,
    gain_second,
    gate_first,
    up_first,
    down_first,
    gate_second,
    up_second,
    down_second,
    out,
    w_in,
    w_down,
    normed,
    own,
    part_out,
    part_in,
    hidden,
    total,
    rs_own,
    rs_out,
    rs_in,
    merged,
    sq_own,
    sq_out,
    sq_in,
    scale,
    w_sem,
    part_send,
    part_recv,
    hid_send,
    hid_recv,
    sq_send,
    sq_recv,
    rs_send,
    rs_recv,
    ag_send,
    ag_recv,
):
    R, C, blocks, pieces, width, half_rows, gap, model = cfg
    rows = 2 * half_rows
    per_phase = blocks * pieces
    count = 2 * per_phase
    r = lax.axis_index("ra")
    c = lax.axis_index("cb")

    gates, ups, downs = (gate_first, gate_second), (up_first, up_second), (down_first, down_second)

    def weight_copy(phase, p, which):
        span = pl.ds(p * width, width)
        if which == 2:
            return pltpu.make_async_copy(
                downs[phase].at[span, :], w_down.at[phase, p], w_sem.at[phase, 2, p]
            )
        source = (gates, ups)[which][phase]
        return pltpu.make_async_copy(
            source.at[:, span], w_in.at[phase, p, which], w_sem.at[phase, which, p]
        )

    for p in range(pieces):
        weight_copy(0, p, 0).start()
        weight_copy(0, p, 1).start()

    def load_rest(s):
        @pl.when(s == 2)
        def _():
            for p in range(pieces):
                weight_copy(0, p, 2).start()

        @pl.when(s == 6)
        def _():
            for p in range(pieces):
                weight_copy(1, p, 0).start()
                weight_copy(1, p, 1).start()
            for p in range(pieces):
                weight_copy(1, p, 2).start()

    barrier = pltpu.get_barrier_semaphore()

    @pl.when(r > 0)
    def _():
        pl.semaphore_signal(barrier, inc=1, device_id={"ra": r - 1}, device_id_type=MESH)

    @pl.when(r < R - 1)
    def _():
        pl.semaphore_signal(barrier, inc=1, device_id={"ra": r + 1}, device_id_type=MESH)

    for k in range(1, C):
        pl.semaphore_signal(
            barrier, inc=1, device_id={"cb": lax.rem(c + k, C)}, device_id_type=MESH
        )

    def diagonal():
        shape = (half_rows, half_rows)
        return lax.broadcasted_iota(jnp.int32, shape, 0) == lax.broadcasted_iota(jnp.int32, shape, 1)

    def prepare(phase, block, stream, gain_ref):
        values = stream.astype(jnp.float32)
        square = jnp.sum(values * values, axis=1, keepdims=True)
        gain = gain_ref[...].astype(jnp.float32).reshape(1, -1)
        normed[phase, block] = (values * gain).astype(jnp.bfloat16)
        for d in range(2):
            column = square[d * half_rows : (d + 1) * half_rows]
            line = jnp.sum(jnp.where(diagonal(), column, 0.0), axis=0, keepdims=True)
            sq_own[phase, block, d] = jnp.broadcast_to(line, (TILE, half_rows))

    def first(block):
        prepare(0, block, residual[block].reshape(rows, -1), gain_first)

    first(0)

    near = jnp.where(r > 0, 1, 0) + jnp.where(r < R - 1, 1, 0)
    pl.semaphore_wait(barrier, C - 1 + near)

    place = (r, R - 1 - r)
    onward = (r + 1, r - 1)
    back = (r - 1, r + 1)

    def part_copy(d, i):
        return pltpu.make_async_remote_copy(
            src_ref=part_out.at[i, d],
            dst_ref=part_in.at[i, d],
            send_sem=part_send.at[d, i],
            recv_sem=part_recv.at[d, i],
            device_id={"ra": onward[d]},
            device_id_type=MESH,
        )

    def square_copy(d, pb):
        return pltpu.make_async_remote_copy(
            src_ref=sq_out.at[pb, d],
            dst_ref=sq_in.at[pb, d],
            send_sem=sq_send.at[d, pb],
            recv_sem=sq_recv.at[d, pb],
            device_id={"ra": onward[d]},
            device_id_type=MESH,
        )

    def hidden_copy(d, i):
        return pltpu.make_async_remote_copy(
            src_ref=hidden.at[i, d],
            dst_ref=hidden.at[i, d],
            send_sem=hid_send.at[d, i],
            recv_sem=hid_recv.at[d, i],
            device_id={"ra": back[d]},
            device_id_type=MESH,
        )

    def reduce_copy(pb, k):
        peer = lax.rem(c + k, C)
        return pltpu.make_async_remote_copy(
            src_ref=rs_out.at[pb, peer],
            dst_ref=rs_in.at[pb, k - 1],
            send_sem=rs_send.at[pb, k - 1],
            recv_sem=rs_recv.at[pb, k - 1],
            device_id={"cb": peer},
            device_id_type=MESH,
        )

    def spread_copy(pb, k):
        return pltpu.make_async_remote_copy(
            src_ref=merged.at[pb, c],
            dst_ref=merged.at[pb, c],
            send_sem=ag_send.at[pb, k - 1],
            recv_sem=ag_recv.at[pb, k - 1],
            device_id={"cb": lax.rem(c + k, C)},
            device_id_type=MESH,
        )

    def at_step(slot, body):
        early = (slot >= 0) & (slot < per_phase)
        late = (slot >= per_phase + gap) & (slot < count + gap)

        @pl.when(early | late)
        def _():
            phase = jnp.where(late, 1, 0)
            i = slot - phase * gap
            local = i - phase * per_phase
            block = lax.div(local, pieces)
            p = lax.rem(local, pieces)
            body(i, phase, block, p)

    def both_phases(phase, body):
        for static in range(2):

            @pl.when(phase == static)
            def _():
                body(static)

    def project(i, phase, block, p):
        @pl.when(block == 0)
        def _():
            def waits(static):
                weight_copy(static, p, 0).wait()
                weight_copy(static, p, 1).wait()

            both_phases(phase, waits)

        slot = i - phase * per_phase
        x = normed[phase, block]
        for which in range(2):
            product = jnp.dot(x, w_in[phase, p, which], preferred_element_type=jnp.float32)
            own[slot, 0, which] = product[:half_rows]
            own[slot, 1, which] = product[half_rows:]

    def forward(d):
        def body(i, phase, block, p):
            slot = i - phase * per_phase
            pb = phase * blocks + block

            @pl.when(place[d] == 0)
            def _():
                part_out[i, d] = own[slot, d].astype(jnp.bfloat16)
                part_copy(d, i).start()

                @pl.when(p == 0)
                def _():
                    sq_out[pb, d] = sq_own[phase, block, d]
                    square_copy(d, pb).start()

            @pl.when((place[d] > 0) & (place[d] < R - 1))
            def _():
                part_copy(d, i).wait_recv()
                part_out[i, d] = (own[slot, d] + part_in[i, d].astype(jnp.float32)).astype(
                    jnp.bfloat16
                )
                part_copy(d, i).start()

                @pl.when(p == 0)
                def _():
                    square_copy(d, pb).wait_recv()
                    sq_out[pb, d] = sq_own[phase, block, d] + sq_in[pb, d]
                    square_copy(d, pb).start()

            @pl.when(place[d] == R - 1)
            def _():
                @pl.when(p == 0)
                def _():
                    square_copy(d, pb).wait_recv()
                    mean = (sq_own[phase, block, d] + sq_in[pb, d])[:1] / model
                    line = lax.rsqrt(mean + epsilon)
                    column = jnp.sum(jnp.where(diagonal(), line, 0.0), axis=1, keepdims=True)
                    scale[d] = jnp.broadcast_to(column, (half_rows, LANES))

                part_copy(d, i).wait_recv()
                factor = scale[d][:, :1]
                gate = (own[slot, d, 0] + part_in[i, d, 0].astype(jnp.float32)) * factor
                up = (own[slot, d, 1] + part_in[i, d, 1].astype(jnp.float32)) * factor
                hidden[i, d] = (gate / (1.0 + jnp.exp(-gate)) * up).astype(jnp.bfloat16)
                hidden_copy(d, i).start()

        return body

    def pass_back(d):
        def body(i, phase, block, p):
            @pl.when(place[d] < R - 1)
            def _():
                hidden_copy(d, i).wait_recv()

                @pl.when(place[d] > 0)
                def _():
                    hidden_copy(d, i).start()

        return body

    def down(i, phase, block, p):
        @pl.when(block == 0)
        def _():
            both_phases(phase, lambda static: weight_copy(static, p, 2).wait())

        product = jnp.dot(
            hidden[i].reshape(rows, width), w_down[phase, p], preferred_element_type=jnp.float32
        ).reshape(total.shape)

        @pl.when(p == 0)
        def _():
            total[...] = product

        @pl.when(p > 0)
        def _():
            total[...] += product

        @pl.when(p == pieces - 1)
        def _():
            pb = phase * blocks + block
            rs_own[pb] = total[c]
            rs_out[pb] = total[...].astype(jnp.bfloat16)
            for k in range(1, C):
                reduce_copy(pb, k).start()

    def reduce(i, phase, block, p):
        @pl.when(p == pieces - 1)
        def _():
            pb = phase * blocks + block
            branch = rs_own[pb]
            for k in range(1, C):
                reduce_copy(pb, k).wait_recv()
                branch = branch + rs_in[pb, k - 1].astype(jnp.float32)

            @pl.when(phase == 0)
            def _():
                values = residual[block, c].astype(jnp.float32)
                merged[pb, c] = (values + 0.5 * branch).astype(jnp.bfloat16)

            @pl.when(phase == 1)
            def _():
                values = merged[block, c].astype(jnp.float32)
                merged[pb, c] = (values + 0.5 * branch).astype(jnp.bfloat16)

            for k in range(1, C):
                spread_copy(pb, k).start()

    def spread(i, phase, block, p):
        @pl.when(p == pieces - 1)
        def _():
            pb = phase * blocks + block
            for k in range(1, C):
                spread_copy(pb, k).wait_recv()

            @pl.when(phase == 0)
            def _():
                prepare(1, block, merged[pb].reshape(rows, -1), gain_second)

            @pl.when(phase == 1)
            def _():
                out[block] = merged[pb]

    reach = HOP * (R - 1)
    end = 2 * reach

    def step(s, carry):
        load_rest(s)
        for d in range(2):
            at_step(s - 1 - HOP * place[d], forward(d))
        for d in range(2):
            at_step(s - 1 - reach - HOP * (R - 1 - place[d]), pass_back(d))
        at_step(s - 1 - end, down)
        at_step(s - 1 - end - REDUCE, reduce)
        at_step(s - 1 - end - REDUCE - SPREAD, spread)

        @pl.when(s + 1 < blocks)
        def _():
            first(s + 1)

        at_step(s, project)
        return carry

    lax.fori_loop(0, count + gap + end + REDUCE + SPREAD + 1, step, 0)

    def finish(i, carry):
        for d in range(2):

            @pl.when(place[d] < R - 1)
            def _():
                part_copy(d, i).wait_send()

            @pl.when(place[d] > 0)
            def _():
                hidden_copy(d, i).wait_send()

        return carry

    lax.fori_loop(0, count, finish, 0)

    def finish_block(pb, carry):
        for d in range(2):

            @pl.when(place[d] < R - 1)
            def _():
                square_copy(d, pb).wait_send()

        for k in range(1, C):
            reduce_copy(pb, k).wait_send()
            spread_copy(pb, k).wait_send()
        return carry

    lax.fori_loop(0, 2 * blocks, finish_block, 0)


def solution(mesh):
    R, C = mesh.shape["ra"], mesh.shape["cb"]

    def per_device(
        residual,
        gain_first,
        gate_first,
        up_first,
        down_first,
        gain_second,
        gate_second,
        up_second,
        down_second,
    ):
        tokens, depth = residual.shape
        units = gate_first.shape[1]
        blocks = max(1, min(4, tokens // (16 * C)))
        width = 2 * LANES if units % (2 * LANES) == 0 else units
        pieces = units // width
        rows = tokens // blocks
        half_rows = rows // 2
        share = rows // C
        count = 2 * blocks * pieces
        end = 1 + 2 * HOP * (R - 1) + REDUCE + SPREAD
        gap = max(0, pieces - 1 + end - blocks * pieces)
        bf16, f32 = jnp.bfloat16, jnp.float32
        vmem = functools.partial(pl.BlockSpec, memory_space=pltpu.VMEM)
        hbm = functools.partial(pl.BlockSpec, memory_space=pl.ANY)
        pbs = 2 * blocks
        dma = pltpu.SemaphoreType.DMA
        result = pl.pallas_call(
            functools.partial(
                kernel, (R, C, blocks, pieces, width, half_rows, gap, float(depth * R))
            ),
            out_shape=jax.ShapeDtypeStruct((blocks, C, share, depth), bf16),
            in_specs=[vmem()] * 3 + [hbm()] * 6,
            out_specs=vmem(),
            scratch_shapes=[
                pltpu.VMEM((2, pieces, 2, depth, width), bf16),
                pltpu.VMEM((2, pieces, width, depth), bf16),
                pltpu.VMEM((2, blocks, rows, depth), bf16),
                pltpu.VMEM((blocks * pieces, 2, 2, half_rows, width), f32),
                pltpu.VMEM((count, 2, 2, half_rows, width), bf16),
                pltpu.VMEM((count, 2, 2, half_rows, width), bf16),
                pltpu.VMEM((count, 2, half_rows, width), bf16),
                pltpu.VMEM((C, share, depth), f32),
                pltpu.VMEM((pbs, share, depth), f32),
                pltpu.VMEM((pbs, C, share, depth), bf16),
                pltpu.VMEM((pbs, C - 1, share, depth), bf16),
                pltpu.VMEM((pbs, C, share, depth), bf16),
                pltpu.VMEM((2, blocks, 2, TILE, half_rows), f32),
                pltpu.VMEM((pbs, 2, TILE, half_rows), f32),
                pltpu.VMEM((pbs, 2, TILE, half_rows), f32),
                pltpu.VMEM((2, half_rows, LANES), f32),
                dma((2, 3, pieces)),
                dma((2, count)),
                dma((2, count)),
                dma((2, count)),
                dma((2, count)),
                dma((2, pbs)),
                dma((2, pbs)),
                dma((pbs, C - 1)),
                dma((pbs, C - 1)),
                dma((pbs, C - 1)),
                dma((pbs, C - 1)),
            ],
            compiler_params=pltpu.CompilerParams(
                collective_id=0, has_side_effects=True, vmem_limit_bytes=67043328
            ),
        )(
            residual.reshape(blocks, C, share, depth),
            gain_first,
            gain_second,
            gate_first,
            up_first,
            down_first,
            gate_second,
            up_second,
            down_second,
        )
        return result.reshape(tokens, depth)

    in_specs = (
        P("grp", "ra"),
        P("ra"),
        P("ra", "cb"),
        P("ra", "cb"),
        P("cb", "ra"),
        P("ra"),
        P("ra", "cb"),
        P("ra", "cb"),
        P("cb", "ra"),
    )
    return jax.shard_map(
        per_device, mesh=mesh, in_specs=in_specs, out_specs=P("grp", "ra"), check_vma=False
    )
```

profile of v0, /device:TPU:0, one launch (start us, length us, event | category | flops | bytes accessed | tf_op | source)
XLA Modules:
  0.0 131.8 jit_solution(7813382287150585146)
XLA Ops:
  0.0 129.9 %shard_map.91 = bf16[4,4,16,1024]{3,2,1,0:T(8,128)(2,1)} custom-call(bf16[4,4,16,1024]{3,2,1,0:T(8,128)(2,1)} %bitcast.3, bf16[1024]{0:T(1024)(128)(2,1)} %gain_first.1, bf16[1024]{0:T(1024)(128)(2,1)} %gain_second.1, bf16[1024,2816]{1,0:T(8,128)(2,1)} %gate_first.1, bf16[1024,2816]{1,0:T(8,128)(2,1)} %up_first.1, bf16[2816,1024]{1,0:T(8,128)(2,1)} %down_first.1, ...), custom_call_target="tpu_custom_call" | custom-call | tf_op jit(solution)/shard_map/pallas_call | solution.py:430
  129.9 1.9 %copy.11 = bf16[256,1024]{1,0:T(8,128)(2,1)} copy(bf16[256,1024]{1,0:T(8,128)(2,1)} %bitcast.2) | data formatting | bytes 1048576
where the time goes:
time: 132 us
  Pallas kernels  130 us (98%)
  local copies, waits for them, and re-layouts  1.87 us (1%)
    pallas_call x1, Pallas kernels, per_device(): pl.pallas_call(functools.partial(kernel, (R, C, blocks, pieces, width, ha...  130 us

commit v1 on v0

v1 whole, which is shorter than its diff:
```python
import functools

import jax
import jax.numpy as jnp
from jax import lax
from jax.experimental import pallas as pl
from jax.experimental.pallas import tpu as pltpu
from jax.sharding import PartitionSpec as P

MESH = pl.DeviceIdType.MESH
LANES = 128
epsilon = 1e-06

HOP = 4
REDUCE = 4
SPREAD = 4
TILE = 8
AHEAD = 3
LOADS = 6
BEHIND = 4
WIDE = 2
DEEP = 4


def kernel(
    cfg,
    residual,
    gain_first,
    gain_second,
    gate_first,
    up_first,
    down_first,
    gate_second,
    up_second,
    down_second,
    out,
    w_in,
    w_down,
    stream_in,
    normed_one,
    normed,
    own,
    part_out,
    part_in,
    hidden,
    total,
    rs_own,
    rs_out,
    rs_in,
    merged,
    sq_own,
    sq_out,
    sq_in,
    scale,
    w_sem,
    x_sem,
    out_sem,
    part_send,
    part_recv,
    hid_send,
    hid_recv,
    sq_send,
    sq_recv,
    rs_send,
    rs_recv,
    ag_send,
    ag_recv,
):
    R, C, blocks, pieces, width, rows, gap, model = cfg
    per_phase = blocks * pieces
    count = 2 * per_phase
    r = lax.axis_index("ra")
    c = lax.axis_index("cb")

    gates, ups, downs = (gate_first, gate_second), (up_first, up_second), (down_first, down_second)

    def weight_copy(phase, p, which):
        span = pl.ds(p * width if pieces > 1 else 0, width)
        if which == 2:
            return pltpu.make_async_copy(
                downs[phase].at[span, :], w_down.at[phase, p], w_sem.at[phase, 2, p]
            )
        source = (gates, ups)[which][phase]
        return pltpu.make_async_copy(
            source.at[:, span], w_in.at[phase, p, which], w_sem.at[phase, which, p]
        )

    stream_copy = pltpu.make_async_copy(residual, stream_in, x_sem)
    stream_copy.start()
    for p in range(min(AHEAD, pieces)):
        weight_copy(0, p, 0).start()
        weight_copy(0, p, 1).start()

    def load_rest(s):
        def at(first_step, first_piece, phase, kinds):
            p = s - first_step + first_piece

            @pl.when((p >= first_piece) & (p < pieces))
            def _():
                for which in kinds:
                    weight_copy(phase, p, which).start()

        at(0, AHEAD, 0, (0, 1))
        at(LOADS, 0, 0, (2,))
        at(LOADS + pieces, 0, 1, (0, 1))
        at(LOADS + 2 * pieces, 0, 1, (2,))

    barrier = pltpu.get_barrier_semaphore()

    @pl.when(r > 0)
    def _():
        pl.semaphore_signal(barrier, inc=1, device_id={"ra": r - 1}, device_id_type=MESH)

    @pl.when(r < R - 1)
    def _():
        pl.semaphore_signal(barrier, inc=1, device_id={"ra": r + 1}, device_id_type=MESH)

    for k in range(1, C):
        pl.semaphore_signal(
            barrier, inc=1, device_id={"cb": lax.rem(c + k, C)}, device_id_type=MESH
        )

    def diagonal():
        shape = (rows, rows)
        return lax.broadcasted_iota(jnp.int32, shape, 0) == lax.broadcasted_iota(jnp.int32, shape, 1)

    def scaled(stream, gain_ref):
        values = stream.astype(jnp.float32)
        square = jnp.sum(values * values, axis=1, keepdims=True)
        gain = gain_ref[...].astype(jnp.float32).reshape(1, -1)
        return (values * gain).astype(jnp.bfloat16), square

    def keep_square(phase, block, square):
        line = jnp.sum(jnp.where(diagonal(), square, 0.0), axis=0, keepdims=True)
        sq_own[phase, block] = jnp.broadcast_to(line, (TILE, rows))

    stream_copy.wait()
    for block in range(blocks):
        normed_one[pl.ds(block * rows, rows)], square = scaled(
            stream_in[block].reshape(rows, -1), gain_first
        )
        keep_square(0, block, square)

    near = jnp.where(r > 0, 1, 0) + jnp.where(r < R - 1, 1, 0)
    pl.semaphore_wait(barrier, C - 1 + near)

    place = (r, R - 1 - r)
    onward = (r + 1, r - 1)
    back = (r - 1, r + 1)

    def part_copy(d, i):
        return pltpu.make_async_remote_copy(
            src_ref=part_out.at[i],
            dst_ref=part_in.at[i],
            send_sem=part_send.at[i],
            recv_sem=part_recv.at[i],
            device_id={"ra": onward[d]},
            device_id_type=MESH,
        )

    def square_copy(d, pb):
        return pltpu.make_async_remote_copy(
            src_ref=sq_out.at[pb, d],
            dst_ref=sq_in.at[pb, d],
            send_sem=sq_send.at[d, pb],
            recv_sem=sq_recv.at[d, pb],
            device_id={"ra": onward[d]},
            device_id_type=MESH,
        )

    def hidden_copy(d, i):
        return pltpu.make_async_remote_copy(
            src_ref=hidden.at[i],
            dst_ref=hidden.at[i],
            send_sem=hid_send.at[i],
            recv_sem=hid_recv.at[i],
            device_id={"ra": back[d]},
            device_id_type=MESH,
        )

    def squares_went(d, pb):
        return (pieces > 1) | (lax.rem(pb, 2) == d)

    def reduce_copy(pb, k):
        peer = lax.rem(c + k, C)
        return pltpu.make_async_remote_copy(
            src_ref=rs_out.at[pb, peer],
            dst_ref=rs_in.at[pb, k - 1],
            send_sem=rs_send.at[pb, k - 1],
            recv_sem=rs_recv.at[pb, k - 1],
            device_id={"cb": peer},
            device_id_type=MESH,
        )

    def spread_copy(pb, k):
        return pltpu.make_async_remote_copy(
            src_ref=merged.at[pb, c],
            dst_ref=merged.at[pb, c],
            send_sem=ag_send.at[pb, k - 1],
            recv_sem=ag_recv.at[pb, k - 1],
            device_id={"cb": lax.rem(c + k, C)},
            device_id_type=MESH,
        )

    def out_copy(block):
        return pltpu.make_async_copy(
            merged.at[blocks + block], out.at[block], out_sem.at[block]
        )

    def at_step(slot, body, side=None):
        early = (slot >= 0) & (slot < per_phase)
        late = (slot >= per_phase + gap) & (slot < count + gap)

        @pl.when(early | late)
        def _():
            phase = jnp.where(late, 1, 0)
            i = slot - phase * gap
            local = i - phase * per_phase
            block = lax.div(local, pieces)
            p = lax.rem(local, pieces)
            if side is None:
                body(i, phase, block, p)
            else:

                @pl.when(lax.rem(i, 2) == side)
                def _():
                    body(i, phase, block, p)

    def both_phases(phase, body):
        for static in range(2):

            @pl.when(phase == static)
            def _():
                body(static)

    def project_one(s):
        @pl.when(s < pieces)
        def _():
            for which in range(2):
                weight_copy(0, s, which).wait()
            x = normed_one[...]
            for which in range(2):
                product = jnp.dot(x, w_in[0, s, which], preferred_element_type=jnp.float32)
                for block in range(blocks):
                    own[block * pieces + s, which] = product[block * rows : (block + 1) * rows]

    def project_two(s):
        local = s - per_phase - gap

        @pl.when((local >= 0) & (local < per_phase))
        def _():
            block = lax.div(local, pieces)
            p = lax.rem(local, pieces)

            def some(count_of):
                @pl.when(block == 0)
                def _():
                    for q in range(count_of):
                        weight_copy(1, p + q, 0).wait()
                        weight_copy(1, p + q, 1).wait()

                x = normed[block]
                for q in range(count_of):
                    for which in range(2):
                        own[local + q, which] = jnp.dot(
                            x, w_in[1, p + q, which], preferred_element_type=jnp.float32
                        )

            left = pieces % WIDE

            @pl.when((lax.rem(p, WIDE) == 0) & (p + WIDE <= pieces))
            def _():
                some(WIDE)

            if left:

                @pl.when(p == pieces - left)
                def _():
                    some(left)

    def forward(d):
        def body(i, phase, block, p):
            slot = i - phase * per_phase
            pb = phase * blocks + block
            opening = p < 2
            old = i - 2 * BEHIND

            @pl.when((place[d] < R - 1) & (old >= 0))
            def _():
                part_copy(d, old).wait_send()

            @pl.when(place[d] == 0)
            def _():
                part_out[i] = own[slot].astype(jnp.bfloat16)
                part_copy(d, i).start()

                @pl.when(opening)
                def _():
                    sq_out[pb, d] = sq_own[phase, block]
                    square_copy(d, pb).start()

            @pl.when((place[d] > 0) & (place[d] < R - 1))
            def _():
                part_copy(d, i).wait_recv()
                part_out[i] = (own[slot] + part_in[i].astype(jnp.float32)).astype(jnp.bfloat16)
                part_copy(d, i).start()

                @pl.when(opening)
                def _():
                    square_copy(d, pb).wait_recv()
                    sq_out[pb, d] = sq_own[phase, block] + sq_in[pb, d]
                    square_copy(d, pb).start()

            @pl.when(place[d] == R - 1)
            def _():
                @pl.when(opening)
                def _():
                    square_copy(d, pb).wait_recv()
                    mean = (sq_own[phase, block] + sq_in[pb, d])[:1] / model
                    line = lax.rsqrt(mean + epsilon)
                    column = jnp.sum(jnp.where(diagonal(), line, 0.0), axis=1, keepdims=True)
                    scale[d] = jnp.broadcast_to(column, (rows, LANES))

                part_copy(d, i).wait_recv()
                factor = scale[d][:, :1]
                gate = (own[slot, 0] + part_in[i, 0].astype(jnp.float32)) * factor
                up = (own[slot, 1] + part_in[i, 1].astype(jnp.float32)) * factor
                hidden[i] = (gate / (1.0 + jnp.exp(-gate)) * up).astype(jnp.bfloat16)
                hidden_copy(d, i).start()

                @pl.when(old >= 0)
                def _():
                    hidden_copy(d, old).wait_send()

        return body

    def pass_back(d):
        def body(i, phase, block, p):
            @pl.when(place[d] < R - 1)
            def _():
                hidden_copy(d, i).wait_recv()

                @pl.when(place[d] > 0)
                def _():
                    hidden_copy(d, i).start()

                    @pl.when(i >= 2 * BEHIND)
                    def _():
                        hidden_copy(d, i - 2 * BEHIND).wait_send()

        return body

    def down(i, phase, block, p):
        pb = phase * blocks + block

        def some(count_of):
            start = p - count_of + 1
            slot = i - count_of + 1

            @pl.when(block == 0)
            def _():
                for q in range(count_of):
                    both_phases(phase, lambda static: weight_copy(static, start + q, 2).wait())

            product = jnp.dot(
                jnp.concatenate([hidden[slot + q] for q in range(count_of)], axis=1),
                w_down[phase, pl.ds(start, count_of)].reshape(count_of * width, -1),
                preferred_element_type=jnp.float32,
            ).reshape(total.shape)

            @pl.when(start == 0)
            def _():
                total[...] = product

            @pl.when(start > 0)
            def _():
                total[...] += product

        left = pieces % DEEP

        @pl.when(lax.rem(p, DEEP) == DEEP - 1)
        def _():
            some(DEEP)

        if left:

            @pl.when(p == pieces - 1)
            def _():
                some(left)

        @pl.when(p == pieces - 1)
        def _():
            rs_own[pb] = total[c]
            rs_out[pb] = total[...].astype(jnp.bfloat16)
            for k in range(1, C):
                reduce_copy(pb, k).start()
            for d in range(2):

                @pl.when((place[d] < R - 1) & squares_went(d, pb))
                def _():
                    square_copy(d, pb).wait_send()

    def reduce(i, phase, block, p):
        @pl.when(p == pieces - 1)
        def _():
            pb = phase * blocks + block
            branch = rs_own[pb]
            for k in range(1, C):
                reduce_copy(pb, k).wait_recv()
                branch = branch + rs_in[pb, k - 1].astype(jnp.float32)

            @pl.when(phase == 0)
            def _():
                values = stream_in[block, c].astype(jnp.float32)
                merged[pb, c] = (values + 0.5 * branch).astype(jnp.bfloat16)

            @pl.when(phase == 1)
            def _():
                values = merged[block, c].astype(jnp.float32)
                merged[pb, c] = (values + 0.5 * branch).astype(jnp.bfloat16)

            for k in range(1, C):
                spread_copy(pb, k).start()

            @pl.when(pb > 0)
            def _():
                for k in range(1, C):
                    reduce_copy(pb - 1, k).wait_send()
                    spread_copy(pb - 1, k).wait_send()

    def spread(i, phase, block, p):
        @pl.when(p == pieces - 1)
        def _():
            pb = phase * blocks + block
            for k in range(1, C):
                spread_copy(pb, k).wait_recv()

            @pl.when(phase == 0)
            def _():
                normed[block], square = scaled(merged[pb].reshape(rows, -1), gain_second)
                keep_square(1, block, square)

            @pl.when(phase == 1)
            def _():
                out_copy(block).start()

    reach = HOP * (R - 1)
    end = 2 * reach

    def step(s, carry):
        load_rest(s)
        for d in range(2):
            at_step(s - 1 - HOP * place[d], forward(d), d)
        for d in range(2):
            at_step(s - 1 - reach - HOP * (R - 1 - place[d]), pass_back(d), d)
        at_step(s - 1 - end, down)
        at_step(s - 1 - end - REDUCE, reduce)
        at_step(s - 1 - end - REDUCE - SPREAD, spread)

        project_one(s)
        project_two(s)
        return carry

    lax.fori_loop(0, count + gap + end + REDUCE + SPREAD + 1, step, 0)

    for i in range(max(0, count - 2 * BEHIND), count):
        d = i % 2

        @pl.when(place[d] < R - 1)
        def _(d=d, i=i):
            part_copy(d, i).wait_send()

        @pl.when(place[d] > 0)
        def _(d=d, i=i):
            hidden_copy(d, i).wait_send()

    for k in range(1, C):
        reduce_copy(2 * blocks - 1, k).wait_send()
        spread_copy(2 * blocks - 1, k).wait_send()
    for block in range(blocks):
        out_copy(block).wait()


def solution(mesh):
    R, C = mesh.shape["ra"], mesh.shape["cb"]

    def per_device(
        residual,
        gain_first,
        gate_first,
        up_first,
        down_first,
        gain_second,
        gate_second,
        up_second,
        down_second,
    ):
        tokens, depth = residual.shape
        units = gate_first.shape[1]
        blocks = max(1, min(4, tokens // (16 * C)))
        width = 2 * LANES if units % (2 * LANES) == 0 else units
        pieces = units // width
        rows = tokens // blocks
        share = rows // C
        count = 2 * blocks * pieces
        end = 1 + 2 * HOP * (R - 1) + REDUCE + SPREAD
        gap = max(0, pieces - 1 + end - blocks * pieces)
        bf16, f32 = jnp.bfloat16, jnp.float32
        vmem = functools.partial(pl.BlockSpec, memory_space=pltpu.VMEM)
        hbm = functools.partial(pl.BlockSpec, memory_space=pl.ANY)
        pbs = 2 * blocks
        dma = pltpu.SemaphoreType.DMA
        result = pl.pallas_call(
            functools.partial(
                kernel, (R, C, blocks, pieces, width, rows, gap, float(depth * R))
            ),
            out_shape=jax.ShapeDtypeStruct((blocks, C, share, depth), bf16),
            in_specs=[hbm()] + [vmem()] * 2 + [hbm()] * 6,
            out_specs=hbm(),
            scratch_shapes=[
                pltpu.VMEM((2, pieces, 2, depth, width), bf16),
                pltpu.VMEM((2, pieces, width, depth), bf16),
                pltpu.VMEM((blocks, C, share, depth), bf16),
                pltpu.VMEM((tokens, depth), bf16),
                pltpu.VMEM((blocks, rows, depth), bf16),
                pltpu.VMEM((blocks * pieces, 2, rows, width), f32),
                pltpu.VMEM((count, 2, rows, width), bf16),
                pltpu.VMEM((count, 2, rows, width), bf16),
                pltpu.VMEM((count, rows, width), bf16),
                pltpu.VMEM((C, share, depth), f32),
                pltpu.VMEM((pbs, share, depth), f32),
                pltpu.VMEM((pbs, C, share, depth), bf16),
                pltpu.VMEM((pbs, C - 1, share, depth), bf16),
                pltpu.VMEM((pbs, C, share, depth), bf16),
                pltpu.VMEM((2, blocks, TILE, rows), f32),
                pltpu.VMEM((pbs, 2, TILE, rows), f32),
                pltpu.VMEM((pbs, 2, TILE, rows), f32),
                pltpu.VMEM((2, rows, LANES), f32),
                dma((2, 3, pieces)),
                dma,
                dma((blocks,)),
                dma((count,)),
                dma((count,)),
                dma((count,)),
                dma((count,)),
                dma((2, pbs)),
                dma((2, pbs)),
                dma((pbs, C - 1)),
                dma((pbs, C - 1)),
                dma((pbs, C - 1)),
                dma((pbs, C - 1)),
            ],
            compiler_params=pltpu.CompilerParams(
                collective_id=0, has_side_effects=True, vmem_limit_bytes=67043328
            ),
        )(
            residual.reshape(blocks, C, share, depth),
            gain_first,
            gain_second,
            gate_first,
            up_first,
            down_first,
            gate_second,
            up_second,
            down_second,
        )
        return result.reshape(tokens, depth)

    in_specs = (
        P("grp", "ra"),
        P("ra"),
        P("ra", "cb"),
        P("ra", "cb"),
        P("cb", "ra"),
        P("ra"),
        P("ra", "cb"),
        P("ra", "cb"),
        P("cb", "ra"),
    )
    return jax.shard_map(
        per_device, mesh=mesh, in_specs=in_specs, out_specs=P("grp", "ra"), check_vma=False
    )
```

time: 132 us -> 130 us (0.985)
  Pallas kernels: 130 us -> 128 us
    pallas_call x1, Pallas kernels: 130 us -> 128 us  [per_device(): pl.pallas_call(functools.partial(kernel, (R, C, blocks, pieces, width, ro...]
where the time goes in v1:
time: 130 us
  Pallas kernels  128 us (98%)
  local copies, waits for them, and re-layouts  1.87 us (1%)
    pallas_call x1, Pallas kernels, per_device(): pl.pallas_call(functools.partial(kernel, (R, C, blocks, pieces, width, ro...  128 us

profile of v1, /device:TPU:0, one launch (start us, length us, event | category | flops | bytes accessed | tf_op | source)
XLA Modules:
  0.0 129.5 jit_solution(15160843745766030451)
XLA Ops:
  0.0 127.7 %shard_map.91 = bf16[4,4,16,1024]{3,2,1,0:T(8,128)(2,1)} custom-call(bf16[4,4,16,1024]{3,2,1,0:T(8,128)(2,1)} %bitcast.3, bf16[1024]{0:T(1024)(128)(2,1)} %gain_first.1, bf16[1024]{0:T(1024)(128)(2,1)} %gain_second.1, bf16[1024,2816]{1,0:T(8,128)(2,1)} %gate_first.1, bf16[1024,2816]{1,0:T(8,128)(2,1)} %up_first.1, bf16[2816,1024]{1,0:T(8,128)(2,1)} %down_first.1, ...), custom_call_target="tpu_custom_call" | custom-call | tf_op jit(solution)/shard_map/pallas_call | solution.py:513
  127.7 1.9 %copy.11 = bf16[256,1024]{1,0:T(8,128)(2,1)} copy(bf16[256,1024]{1,0:T(8,128)(2,1)} %bitcast.2) | data formatting | bytes 1048576

commit v2 on v1

v2 whole, which is shorter than its diff:
```python
import functools
import heapq

import jax
import jax.numpy as jnp
from jax import lax
from jax.experimental import pallas as pl
from jax.experimental.pallas import tpu as pltpu
from jax.sharding import PartitionSpec as P

MESH = pl.DeviceIdType.MESH
LANES = 128
epsilon = 1e-06

TILE = 8
AHEAD = 3
BEHIND = 4
WIDE = 1
DEEP = 3
UNIT = 1.405

FORWARD, BACKWARD, DOWN, PAIR, ACROSS, SETTLE, PROJECT_ONE, PROJECT_TWO, REST = 0, 2, 4, 5, 6, 7, 8, 9, 10
COST = {
    "op": 0.12, "forward": 0.1, "finish": 0.16, "backward": 0.02, "down": 0.16, "project_one": 0.45,
    "project_two": 0.3, "pair": 0.1, "across": 0.1, "settle": 0.2, "hop": 2.2, "near": 1.8, "far": 4.2,
    "queue": 2.0, "bubble": 0.05,
}
RANK = {
    "settle": 0.5, "across": 0.6, "pair": 0.7, "backward0": 2, "forward1": 2.5, "forward0": 3,
    "project_one": 3.6, "down0": 4, "backward1": 4.75, "project_two": 5.2, "down1": 6.4,
}


def plan(R, blocks, pieces, deep, wide, busy, cost=COST, rank=RANK):
    per_phase = blocks * pieces
    count = 2 * per_phase
    heap = []
    ticket = 0
    groups = []
    for pb in range(2 * blocks):
        for start in range(0, pieces, deep):
            groups.append((pb, start, min(deep, pieces - start)))
    wides = []
    for block in range(blocks):
        for start in range(0, pieces, wide):
            wides.append((block, start, min(wide, pieces - start)))
    units = [[i for i in range(count) if i % 2 == d] for d in range(2)]
    nodes = []
    for z in range(R):
        nodes.append(dict(
            time=0.0, own=set(), forward=[0, 0], backward=[0, 0], down=0, pair=0, across=0, settle=0,
            one=0, two=0, sums=set(), hidden=set(), done=set(), near={}, far={}, back={}, order=[],
        ))
    free = {}
    sent = {}

    def poke(time, z):
        nonlocal ticket
        ticket += 1
        heapq.heappush(heap, (time, ticket, "try", z, None))

    def land(time, z, where, key):
        nonlocal ticket
        ticket += 1
        heapq.heappush(heap, (time, ticket, where, z, key))

    for z in range(R):
        poke(0.0, z)
        for p in range(pieces):
            poke(0.3 * (p + 1), z)
    while heap:
        now, _, event, z, key = heapq.heappop(heap)
        node = nodes[z]
        if event != "try":
            if event in ("sums", "hidden"):
                node[event].add(key)
            else:
                node[event][key] = now
        if node["time"] > now + 1e-9:
            continue
        place = (z, R - 1 - z)
        best = None

        def offer(name, kind, value, duration):
            nonlocal best
            if best is None or rank[name] < best[0]:
                best = (rank[name], kind, value, duration)

        wake = []

        def open_link(way):
            until = free.get((z, way), 0.0) - cost["queue"]
            if until > now + 1e-9:
                wake.append(until)
                return False
            return True

        for d in range(2):
            way = 1 - 2 * d
            at = node["forward"][d]
            if at < len(units[d]):
                i = units[d][at]
                if i in node["own"] and (place[d] == 0 or i in node["sums"]):
                    phase = i // per_phase
                    if place[d] == R - 1:
                        offer("forward%d" % phase, FORWARD, i, cost["finish"])
                    elif open_link(way):
                        offer("forward%d" % phase, FORWARD, i, cost["forward"])
            at = node["backward"][d]
            if place[d] > 0 and at < len(units[d]):
                i = units[d][at]
                if i in (node["done"] if place[d] == R - 1 else node["hidden"]) and open_link(-way):
                    offer("backward%d" % (i // per_phase), BACKWARD, i, cost["backward"])
        if node["down"] < len(groups):
            pb, start, size = groups[node["down"]]
            ready = True
            for i in range(pb * pieces + start, pb * pieces + start + size):
                d = i % 2
                if place[d] == 0:
                    ready &= i in node["hidden"]
                elif place[d] == R - 1:
                    ready &= i in node["done"]
                else:
                    ready &= units[d].index(i) < node["backward"][d]
            if ready:
                offer("down%d" % (pb // blocks), DOWN, node["down"], cost["down"] * size)
        for name, kind, source in (("pair", PAIR, "near"), ("across", ACROSS, "far"), ("settle", SETTLE, "back")):
            if node[source].get(node[name], 1e9) <= now + 1e-9:
                offer(name, kind, node[name], cost[name])
        if node["one"] < pieces and 0.3 * (node["one"] + 1) <= now + 1e-9:
            offer("project_one", PROJECT_ONE, node["one"], cost["project_one"])
        if node["two"] < len(wides):
            block, start, size = wides[node["two"]]
            if node["settle"] > block:
                offer("project_two", PROJECT_TWO, block * pieces + start, cost["project_two"] * size)
        if best is None:
            for until in wake:
                poke(until, z)
            continue
        _, kind, value, duration = best
        node["order"].append(kind + value % 2 if kind in (FORWARD, BACKWARD) else kind)
        end = now + cost["op"] + duration
        node["time"] = end

        def send(way, size, where, i):
            begin = max(end, free.get((z, way), 0.0))
            free[(z, way)] = begin + size + cost["bubble"]
            land(free[(z, way)] + cost["hop"], z + way, where, i)

        if kind in (FORWARD, BACKWARD):
            d = value % 2
            way = 1 - 2 * d
            if kind == FORWARD:
                node["forward"][d] += 1
                if place[d] == R - 1:
                    node["done"].add(value)
                else:
                    send(way, busy, "sums", value)
            else:
                node["backward"][d] += 1
                send(-way, busy / 2, "hidden", value)
        elif kind == DOWN:
            pb, start, size = groups[value]
            node["down"] += 1
            if start + size == pieces:
                land(end + cost["near"], z, "near", pb)
        elif kind == PAIR:
            node["pair"] += 1
            land(end + cost["far"], z, "far", value)
        elif kind == ACROSS:
            node["across"] += 1
            land(end + cost["near"], z, "back", value)
        elif kind == SETTLE:
            node["settle"] += 1
        elif kind == PROJECT_ONE:
            node["one"] += 1
            node["own"].update(block * pieces + value for block in range(blocks))
        else:
            block, start, size = wides[node["two"]]
            node["two"] += 1
            node["own"].update(per_phase + value + q for q in range(size))
        poke(end, z)
    for node in nodes:
        assert node["settle"] == 2 * blocks
    orders = [node["order"] for node in nodes]
    return orders


def kernel(
    cfg,
    residual,
    gain_first,
    gain_second,
    gate_first,
    up_first,
    down_first,
    gate_second,
    up_second,
    down_second,
    out,
    w_in,
    w_down,
    stream_in,
    normed_one,
    normed,
    own,
    part_out,
    part_in,
    hidden,
    total,
    table,
    pair_own,
    pair_out,
    pair_in,
    shares,
    merged,
    sq_own,
    sq_out,
    sq_in,
    scale,
    w_sem,
    x_sem,
    part_send,
    part_recv,
    hid_send,
    hid_recv,
    sq_send,
    sq_recv,
    pair_send,
    pair_recv,
    rs_send,
    rs_recv,
    ag_send,
    ag_recv,
):
    R, C, blocks, pieces, width, rows, orders, model = cfg
    per_phase = blocks * pieces
    count = 2 * per_phase
    r = lax.axis_index("ra")
    c = lax.axis_index("cb")
    X = C // 2
    side, spot = lax.rem(c, 2), lax.div(c, 2)
    half = rows // 2
    length = max(len(order) for order in orders)

    gates, ups, downs = (gate_first, gate_second), (up_first, up_second), (down_first, down_second)

    def weight_copy(phase, p, which):
        span = pl.ds(p * width if pieces > 1 else 0, width)
        if which == 2:
            return pltpu.make_async_copy(
                downs[phase].at[span, :], w_down.at[phase, p], w_sem.at[phase, 2, p]
            )
        source = (gates, ups)[which][phase]
        return pltpu.make_async_copy(
            source.at[:, span], w_in.at[phase, p, which], w_sem.at[phase, which, p]
        )

    stream_copy = pltpu.make_async_copy(residual, stream_in, x_sem)
    stream_copy.start()
    for p in range(min(AHEAD, pieces)):
        weight_copy(0, p, 0).start()
        weight_copy(0, p, 1).start()

    for z, order in enumerate(orders):

        @pl.when(r == z)
        def _(order=order):
            for at, kind in enumerate(order):
                table[at] = kind
            for at in range(len(order), length):
                table[at] = REST

    barrier = pltpu.get_barrier_semaphore()

    @pl.when(r > 0)
    def _():
        pl.semaphore_signal(barrier, inc=1, device_id={"ra": r - 1}, device_id_type=MESH)

    @pl.when(r < R - 1)
    def _():
        pl.semaphore_signal(barrier, inc=1, device_id={"ra": r + 1}, device_id_type=MESH)

    for k in range(1, C):
        pl.semaphore_signal(
            barrier, inc=1, device_id={"cb": lax.rem(c + k, C)}, device_id_type=MESH
        )

    def diagonal():
        shape = (rows, rows)
        return lax.broadcasted_iota(jnp.int32, shape, 0) == lax.broadcasted_iota(jnp.int32, shape, 1)

    def scaled(stream, gain_ref):
        values = stream.astype(jnp.float32)
        square = jnp.sum(values * values, axis=1, keepdims=True)
        gain = gain_ref[...].astype(jnp.float32).reshape(1, -1)
        return (values * gain).astype(jnp.bfloat16), square

    def keep_square(phase, block, square):
        line = jnp.sum(jnp.where(diagonal(), square, 0.0), axis=0, keepdims=True)
        sq_own[phase, block] = jnp.broadcast_to(line, (TILE, rows))

    stream_copy.wait()
    for block in range(blocks):
        normed_one[pl.ds(block * rows, rows)], square = scaled(
            stream_in[block].reshape(rows, -1), gain_first
        )
        keep_square(0, block, square)

    near = jnp.where(r > 0, 1, 0) + jnp.where(r < R - 1, 1, 0)
    pl.semaphore_wait(barrier, C - 1 + near)

    def of_side(d):
        rise = d == 0
        place = jnp.where(rise, r, R - 1 - r)
        return place, jnp.where(rise, r + 1, r - 1), jnp.where(rise, r - 1, r + 1)

    def part_copy(i):
        return pltpu.make_async_remote_copy(
            src_ref=part_out.at[i],
            dst_ref=part_in.at[i],
            send_sem=part_send.at[i],
            recv_sem=part_recv.at[i],
            device_id={"ra": of_side(lax.rem(i, 2))[1]},
            device_id_type=MESH,
        )

    def square_copy(d, pb):
        return pltpu.make_async_remote_copy(
            src_ref=sq_out.at[pb, d],
            dst_ref=sq_in.at[pb, d],
            send_sem=sq_send.at[d, pb],
            recv_sem=sq_recv.at[d, pb],
            device_id={"ra": of_side(d)[1]},
            device_id_type=MESH,
        )

    def hidden_copy(i):
        return pltpu.make_async_remote_copy(
            src_ref=hidden.at[i],
            dst_ref=hidden.at[i],
            send_sem=hid_send.at[i],
            recv_sem=hid_recv.at[i],
            device_id={"ra": of_side(lax.rem(i, 2))[2]},
            device_id_type=MESH,
        )

    def squares_went(d, pb):
        return (pieces > 1) | (lax.rem(pb, 2) == d)

    def pair_copy(pb):
        return pltpu.make_async_remote_copy(
            src_ref=pair_out.at[pb],
            dst_ref=pair_in.at[pb],
            send_sem=pair_send.at[pb],
            recv_sem=pair_recv.at[pb],
            device_id={"cb": c + 1 - 2 * side},
            device_id_type=MESH,
        )

    def across_copy(pb, k):
        return pltpu.make_async_remote_copy(
            src_ref=shares.at[pb, spot],
            dst_ref=shares.at[pb, spot],
            send_sem=rs_send.at[pb, k - 1],
            recv_sem=rs_recv.at[pb, k - 1],
            device_id={"cb": 2 * lax.rem(spot + k, X) + side},
            device_id_type=MESH,
        )

    def spread_copy(pb):
        return pltpu.make_async_remote_copy(
            src_ref=merged.at[pb, side],
            dst_ref=merged.at[pb, side],
            send_sem=ag_send.at[pb],
            recv_sem=ag_recv.at[pb],
            device_id={"cb": c + 1 - 2 * side},
            device_id_type=MESH,
        )

    def unit_of(i):
        phase = jnp.where(i >= per_phase, 1, 0)
        local = i - phase * per_phase
        return phase, lax.div(local, pieces), lax.rem(local, pieces)

    def project_one(p):
        @pl.when(p + AHEAD < pieces)
        def _():
            weight_copy(0, p + AHEAD, 0).start()
            weight_copy(0, p + AHEAD, 1).start()

        weight_copy(0, p, 2).start()
        for which in range(2):
            weight_copy(0, p, which).wait()
        x = normed_one[...]
        for which in range(2):
            product = jnp.dot(x, w_in[0, p, which], preferred_element_type=jnp.float32)
            for block in range(blocks):
                own[block * pieces + p, which] = product[block * rows : (block + 1) * rows]

    def grouped(p, size, body):
        left = pieces % size
        if left == 0:
            body(size)
        elif left == pieces:
            body(left)
        else:

            @pl.when(p + size <= pieces)
            def _():
                body(size)

            @pl.when(p + size > pieces)
            def _():
                body(left)

    def project_two(local):
        block = lax.div(local, pieces)
        p = lax.rem(local, pieces)

        def some(size):
            @pl.when(block == 0)
            def _():
                for q in range(size):
                    weight_copy(1, p + q, 0).wait()
                    weight_copy(1, p + q, 1).wait()

            x = normed[block]
            for q in range(size):
                for which in range(2):
                    own[local + q, which] = jnp.dot(
                        x, w_in[1, p + q, which], preferred_element_type=jnp.float32
                    )

        grouped(p, WIDE, some)

    def forward(i, d):
        phase, block, p = unit_of(i)
        place = of_side(d)[0]
        slot = i - phase * per_phase
        pb = phase * blocks + block
        opening = p < 2
        old = i - 2 * BEHIND

        @pl.when((place < R - 1) & (old >= 0))
        def _():
            part_copy(old).wait_send()

        @pl.when(place == 0)
        def _():
            part_out[i] = own[slot].astype(jnp.bfloat16)
            part_copy(i).start()

            @pl.when(opening)
            def _():
                sq_out[pb, d] = sq_own[phase, block]
                square_copy(d, pb).start()

        @pl.when((place > 0) & (place < R - 1))
        def _():
            part_copy(i).wait_recv()
            part_out[i] = (own[slot] + part_in[i].astype(jnp.float32)).astype(jnp.bfloat16)
            part_copy(i).start()

            @pl.when(opening)
            def _():
                square_copy(d, pb).wait_recv()
                sq_out[pb, d] = sq_own[phase, block] + sq_in[pb, d]
                square_copy(d, pb).start()

        @pl.when(place == R - 1)
        def _():
            @pl.when(opening)
            def _():
                square_copy(d, pb).wait_recv()
                mean = (sq_own[phase, block] + sq_in[pb, d])[:1] / model
                line = lax.rsqrt(mean + epsilon)
                column = jnp.sum(jnp.where(diagonal(), line, 0.0), axis=1, keepdims=True)
                scale[d] = jnp.broadcast_to(column, (rows, LANES))

            part_copy(i).wait_recv()
            factor = scale[d][:, :1]
            gate = (own[slot, 0] + part_in[i, 0].astype(jnp.float32)) * factor
            up = (own[slot, 1] + part_in[i, 1].astype(jnp.float32)) * factor
            hidden[i] = (gate / (1.0 + jnp.exp(-gate)) * up).astype(jnp.bfloat16)

    def backward(i, d):
        place = of_side(d)[0]

        @pl.when(place < R - 1)
        def _():
            hidden_copy(i).wait_recv()

        hidden_copy(i).start()

        @pl.when(i >= 2 * BEHIND)
        def _():
            hidden_copy(i - 2 * BEHIND).wait_send()

    steps = -(-pieces // DEEP)

    def down(group):
        pb = lax.div(group, steps)
        phase = jnp.where(pb >= blocks, 1, 0)
        start = lax.rem(group, steps) * DEEP

        def some(size):
            for q in range(size):
                i = pb * pieces + start + q

                @pl.when(of_side(lax.rem(i, 2))[0] == 0)
                def _(i=i):
                    hidden_copy(i).wait_recv()

                @pl.when(pb == 0)
                def _(q=q):
                    weight_copy(0, start + q, 2).wait()
                    weight_copy(1, start + q, 0).start()
                    weight_copy(1, start + q, 1).start()
                    weight_copy(1, start + q, 2).start()

                @pl.when(pb == blocks)
                def _(q=q):
                    weight_copy(1, start + q, 2).wait()

            slot = pb * pieces + start
            product = jnp.dot(
                jnp.concatenate([hidden[slot + q] for q in range(size)], axis=1),
                w_down[phase, pl.ds(start, size)].reshape(size * width, -1),
                preferred_element_type=jnp.float32,
            )

            @pl.when(start == 0)
            def _():
                total[...] = product.reshape(total.shape)

            @pl.when(start > 0)
            def _():
                total[...] += product.reshape(total.shape)

        grouped(start, DEEP, some)

        @pl.when(start + DEEP >= pieces)
        def _():
            pair_own[lax.rem(pb, 2)] = total[side]
            pair_out[pb] = total[1 - side]
            pair_copy(pb).start()
            for d in range(2):

                @pl.when((of_side(d)[0] < R - 1) & squares_went(d, pb))
                def _(d=d):
                    square_copy(d, pb).wait_send()

    def pair(pb):
        pair_copy(pb).wait_recv()
        shares[pb, spot] = (pair_own[lax.rem(pb, 2)] + pair_in[pb]).astype(jnp.bfloat16)
        for k in range(1, X):
            across_copy(pb, k).start()

        @pl.when(pb > 0)
        def _():
            pair_copy(pb - 1).wait_send()

    def across(pb):
        for k in range(1, X):
            across_copy(pb, k).wait_recv()
        branch = shares[pb, 0].astype(jnp.float32)
        for x in range(1, X):
            branch = branch + shares[pb, x].astype(jnp.float32)

        @pl.when(pb < blocks)
        def _():
            values = stream_in[pb, side].astype(jnp.float32)
            merged[pb, side] = (values + 0.5 * branch).astype(jnp.bfloat16)

        @pl.when(pb >= blocks)
        def _():
            values = merged[pb - blocks, side].astype(jnp.float32)
            merged[pb, side] = (values + 0.5 * branch).astype(jnp.bfloat16)

        spread_copy(pb).start()

        @pl.when(pb > 0)
        def _():
            for k in range(1, X):
                across_copy(pb - 1, k).wait_send()
            spread_copy(pb - 1).wait_send()

    def settle(pb):
        spread_copy(pb).wait_recv()

        @pl.when(pb < blocks)
        def _():
            normed[pb], square = scaled(merged[pb].reshape(rows, -1), gain_second)
            keep_square(1, pb, square)

        @pl.when(pb >= blocks)
        def _():
            out[pb - blocks] = merged[pb]

    bodies = (
        lambda n: forward(2 * n, 0),
        lambda n: forward(2 * n + 1, 1),
        lambda n: backward(2 * n, 0),
        lambda n: backward(2 * n + 1, 1),
        down,
        pair,
        across,
        settle,
        project_one,
        project_two,
    )

    def step(at, counts):
        what = table[at]

        def one(kind):
            def run():
                bodies[kind](counts[kind])
                return counts[kind] + 1

            return lax.cond(what == kind, run, lambda: counts[kind])

        return tuple(one(kind) for kind in range(len(bodies)))

    lax.fori_loop(0, length, step, (jnp.int32(0),) * len(bodies))

    for i in range(max(0, count - 2 * BEHIND), count):
        place = of_side(i % 2)[0]

        @pl.when(place < R - 1)
        def _(i=i):
            part_copy(i).wait_send()

        @pl.when(place > 0)
        def _(i=i):
            hidden_copy(i).wait_send()

    newest = 2 * blocks - 1
    pair_copy(newest).wait_send()
    for k in range(1, X):
        across_copy(newest, k).wait_send()
    spread_copy(newest).wait_send()


def solution(mesh):
    R, C = mesh.shape["ra"], mesh.shape["cb"]

    def per_device(
        residual,
        gain_first,
        gate_first,
        up_first,
        down_first,
        gain_second,
        gate_second,
        up_second,
        down_second,
    ):
        tokens, depth = residual.shape
        units = gate_first.shape[1]
        blocks = max(1, min(4, tokens // (16 * C)))
        width = 2 * LANES if units % (2 * LANES) == 0 else units
        pieces = units // width
        rows = tokens // blocks
        count = 2 * blocks * pieces
        half = rows // 2
        orders = plan(R, blocks, pieces, DEEP, WIDE, UNIT)
        length = max(len(order) for order in orders)
        bf16, f32 = jnp.bfloat16, jnp.float32
        vmem = functools.partial(pl.BlockSpec, memory_space=pltpu.VMEM)
        hbm = functools.partial(pl.BlockSpec, memory_space=pl.ANY)
        pbs = 2 * blocks
        dma = pltpu.SemaphoreType.DMA
        result = pl.pallas_call(
            functools.partial(
                kernel, (R, C, blocks, pieces, width, rows, orders, float(depth * R))
            ),
            out_shape=pltpu.VMEM((blocks, 2, half, depth), bf16),
            in_specs=[hbm()] + [vmem()] * 2 + [hbm()] * 6,
            out_specs=vmem(),
            scratch_shapes=[
                pltpu.VMEM((2, pieces, 2, depth, width), bf16),
                pltpu.VMEM((2, pieces, width, depth), bf16),
                pltpu.VMEM((blocks, 2, half, depth), bf16),
                pltpu.VMEM((tokens, depth), bf16),
                pltpu.VMEM((blocks, rows, depth), bf16),
                pltpu.VMEM((blocks * pieces, 2, rows, width), f32),
                pltpu.VMEM((count, 2, rows, width), bf16),
                pltpu.VMEM((count, 2, rows, width), bf16),
                pltpu.VMEM((count, rows, width), bf16),
                pltpu.VMEM((2, half, depth), f32),
                pltpu.SMEM((length,), jnp.int32),
                pltpu.VMEM((2, half, depth), f32),
                pltpu.VMEM((pbs, half, depth), f32),
                pltpu.VMEM((pbs, half, depth), f32),
                pltpu.VMEM((pbs, C // 2, half, depth), bf16),
                pltpu.VMEM((pbs, 2, half, depth), bf16),
                pltpu.VMEM((2, blocks, TILE, rows), f32),
                pltpu.VMEM((pbs, 2, TILE, rows), f32),
                pltpu.VMEM((pbs, 2, TILE, rows), f32),
                pltpu.VMEM((2, rows, LANES), f32),
                dma((2, 3, pieces)),
                dma,
                dma((count,)),
                dma((count,)),
                dma((count,)),
                dma((count,)),
                dma((2, pbs)),
                dma((2, pbs)),
                dma((pbs,)),
                dma((pbs,)),
                dma((pbs, max(1, C // 2 - 1))),
                dma((pbs, max(1, C // 2 - 1))),
                dma((pbs,)),
                dma((pbs,)),
            ],
            compiler_params=pltpu.CompilerParams(
                collective_id=0, has_side_effects=True, vmem_limit_bytes=66400000
            ),
        )(
            residual.reshape(blocks, 2, half, depth),
            gain_first,
            gain_second,
            gate_first,
            up_first,
            down_first,
            gate_second,
            up_second,
            down_second,
        )
        return result.reshape(tokens, depth)

    in_specs = (
        P("grp", "ra"),
        P("ra"),
        P("ra", "cb"),
        P("ra", "cb"),
        P("cb", "ra"),
        P("ra"),
        P("ra", "cb"),
        P("ra", "cb"),
        P("cb", "ra"),
    )
    return jax.shard_map(
        per_device, mesh=mesh, in_specs=in_specs, out_specs=P("grp", "ra"), check_vma=False
    )
```

time: 130 us -> 127 us (0.977)
  Pallas kernels: 128 us -> 126 us
    pallas_call x1, Pallas kernels: 128 us -> 126 us  [per_device(): pl.pallas_call(functools.partial(kernel, (R, C, blocks, pieces, width, ro...]
where the time goes in v2:
time: 127 us
  Pallas kernels  126 us (99%)
    pallas_call x1, Pallas kernels, per_device(): pl.pallas_call(functools.partial(kernel, (R, C, blocks, pieces, width, ro...  126 us

profile of v2, /device:TPU:0, one launch (start us, length us, event | category | flops | bytes accessed | tf_op | source)
XLA Modules:
  0.0 127.2 jit_solution(9376777118959526457)
XLA Ops:
  0.0 126.4 %shard_map.91 = bf16[4,2,32,1024]{3,2,1,0:T(8,128)(2,1)S(1)} custom-call(bf16[4,2,32,1024]{3,2,1,0:T(8,128)(2,1)} %bitcast.3, bf16[1024]{0:T(1024)(128)(2,1)} %gain_first.1, bf16[1024]{0:T(1024)(128)(2,1)} %gain_second.1, bf16[1024,2816]{1,0:T(8,128)(2,1)} %gate_first.1, bf16[1024,2816]{1,0:T(8,128)(2,1)} %up_first.1, bf16[2816,1024]{1,0:T(8,128)(2,1)} %down_first.1, ...), custom_call_target="tpu_custom_call" | custom-call | tf_op jit(solution)/shard_map/pallas_call | solution.py:675
  126.4 0.8 copy.11

commit v3 on v2

--- a/solution.py
+++ b/solution.py
@@ -16,7 +16,8 @@
 AHEAD = 3
 BEHIND = 4
 WIDE = 1
-DEEP = 3
+FIRST = 2
+DEEP = 4
 UNIT = 1.405
 
 FORWARD, BACKWARD, DOWN, PAIR, ACROSS, SETTLE, PROJECT_ONE, PROJECT_TWO, REST = 0, 2, 4, 5, 6, 7, 8, 9, 10
@@ -48,8 +49,8 @@
     nodes = []
     for z in range(R):
         nodes.append(dict(
-            time=0.0, own=set(), forward=[0, 0], backward=[0, 0], down=0, pair=0, across=0, settle=0,
-            one=0, two=0, sums=set(), hidden=set(), done=set(), near={}, far={}, back={}, order=[],
+            time=0.0, own={b * pieces + p for b in range(blocks) for p in range(min(FIRST, pieces))}, forward=[0, 0], backward=[0, 0], down=0, pair=0, across=0, settle=0,
+            one=min(FIRST, pieces), two=0, sums=set(), hidden=set(), done=set(), near={}, far={}, back={}, order=[],
         ))
     free = {}
     sent = {}
@@ -201,6 +202,8 @@
     w_in,
     w_down,
     stream_in,
+    gain_one,
+    gain_two,
     normed_one,
     normed,
     own,
@@ -220,6 +223,7 @@
     scale,
     w_sem,
     x_sem,
+    gain_sem,
     part_send,
     part_recv,
     hid_send,
@@ -258,6 +262,12 @@
 
     stream_copy = pltpu.make_async_copy(residual, stream_in, x_sem)
     stream_copy.start()
+    gain_copies = [
+        pltpu.make_async_copy(source, kept, gain_sem.at[at])
+        for at, (source, kept) in enumerate(((gain_first, gain_one), (gain_second, gain_two)))
+    ]
+    gain_copies[0].start()
+    gain_copies[1].start()
     for p in range(min(AHEAD, pieces)):
         weight_copy(0, p, 0).start()
         weight_copy(0, p, 1).start()
@@ -301,11 +311,31 @@
         sq_own[phase, block] = jnp.broadcast_to(line, (TILE, rows))
 
     stream_copy.wait()
+    gain_copies[0].wait()
+    gain_copies[1].wait()
     for block in range(blocks):
         normed_one[pl.ds(block * rows, rows)], square = scaled(
-            stream_in[block].reshape(rows, -1), gain_first
+            stream_in[block].reshape(rows, -1), gain_one
         )
         keep_square(0, block, square)
+
+    def project_one(p):
+        @pl.when(p + AHEAD < pieces)
+        def _():
+            weight_copy(0, p + AHEAD, 0).start()
+            weight_copy(0, p + AHEAD, 1).start()
+
+        weight_copy(0, p, 2).start()
+        for which in range(2):
+            weight_copy(0, p, which).wait()
+        x = normed_one[...]
+        for which in range(2):
+            product = jnp.dot(x, w_in[0, p, which], preferred_element_type=jnp.float32)
+            for block in range(blocks):
+                own[block * pieces + p, which] = product[block * rows : (block + 1) * rows]
+
+    for p in range(min(FIRST, pieces)):
+        project_one(p)
 
     near = jnp.where(r > 0, 1, 0) + jnp.where(r < R - 1, 1, 0)
     pl.semaphore_wait(barrier, C - 1 + near)
@@ -383,21 +413,6 @@
         local = i - phase * per_phase
         return phase, lax.div(local, pieces), lax.rem(local, pieces)
 
-    def project_one(p):
-        @pl.when(p + AHEAD < pieces)
-        def _():
-            weight_copy(0, p + AHEAD, 0).start()
-            weight_copy(0, p + AHEAD, 1).start()
-
-        weight_copy(0, p, 2).start()
-        for which in range(2):
-            weight_copy(0, p, which).wait()
-        x = normed_one[...]
-        for which in range(2):
-            product = jnp.dot(x, w_in[0, p, which], preferred_element_type=jnp.float32)
-            for block in range(blocks):
-                own[block * pieces + p, which] = product[block * rows : (block + 1) * rows]
-
     def grouped(p, size, body):
         left = pieces % size
         if left == 0:
@@ -591,7 +606,7 @@
 
         @pl.when(pb < blocks)
         def _():
-            normed[pb], square = scaled(merged[pb].reshape(rows, -1), gain_second)
+            normed[pb], square = scaled(merged[pb].reshape(rows, -1), gain_two)
             keep_square(1, pb, square)
 
         @pl.when(pb >= blocks)
@@ -621,9 +636,17 @@
 
             return lax.cond(what == kind, run, lambda: counts[kind])
 
-        return tuple(one(kind) for kind in range(len(bodies)))
-
-    lax.fori_loop(0, length, step, (jnp.int32(0),) * len(bodies))
+        after = []
+        for kinds in (range(2), range(2, 4), range(4, 6), range(6, len(bodies))):
+            after += lax.cond(
+                (what >= kinds[0]) & (what <= kinds[-1]),
+                lambda: tuple(one(kind) for kind in kinds),
+                lambda: tuple(counts[kind] for kind in kinds),
+            )
+        return tuple(after)
+
+    done = [min(FIRST, pieces) if body is project_one else 0 for body in bodies]
+    lax.fori_loop(0, length, step, tuple(jnp.int32(n) for n in done))
 
     for i in range(max(0, count - 2 * BEHIND), count):
         place = of_side(i % 2)[0]
@@ -677,12 +700,14 @@
                 kernel, (R, C, blocks, pieces, width, rows, orders, float(depth * R))
             ),
             out_shape=pltpu.VMEM((blocks, 2, half, depth), bf16),
-            in_specs=[hbm()] + [vmem()] * 2 + [hbm()] * 6,
+            in_specs=[hbm()] * 9,
             out_specs=vmem(),
             scratch_shapes=[
                 pltpu.VMEM((2, pieces, 2, depth, width), bf16),
                 pltpu.VMEM((2, pieces, width, depth), bf16),
                 pltpu.VMEM((blocks, 2, half, depth), bf16),
+                pltpu.VMEM((depth,), bf16),
+                pltpu.VMEM((depth,), bf16),
                 pltpu.VMEM((tokens, depth), bf16),
                 pltpu.VMEM((blocks, rows, depth), bf16),
                 pltpu.VMEM((blocks * pieces, 2, rows, width), f32),
@@ -702,6 +727,7 @@
                 pltpu.VMEM((2, rows, LANES), f32),
                 dma((2, 3, pieces)),
                 dma,
+                dma((2,)),
                 dma((count,)),
                 dma((count,)),
                 dma((count,)),

time: 127 us -> 125 us (0.984)
  Pallas kernels: 126 us -> 124 us
    pallas_call x1, Pallas kernels: 126 us -> 124 us  [per_device(): pl.pallas_call(functools.partial(kernel, (R, C, blocks, pieces, width, ro...]
where the time goes in v3:
time: 125 us; the launch traced here: 124 us
  Pallas kernels  124 us (99%)
    pallas_call x1, Pallas kernels, per_device(): pl.pallas_call(functools.partial(kernel, (R, C, blocks, pieces, width, ro...  124 us

profile of v3, /device:TPU:0, one launch (start us, length us, event | category | flops | bytes accessed | tf_op | source)
XLA Modules:
  0.0 124.5 jit_solution(9535078579907962959)
XLA Ops:
  0.0 123.7 %shard_map.91 = bf16[4,2,32,1024]{3,2,1,0:T(8,128)(2,1)S(1)} custom-call(bf16[4,2,32,1024]{3,2,1,0:T(8,128)(2,1)} %bitcast.3, bf16[1024]{0:T(1024)(128)(2,1)} %gain_first.1, bf16[1024]{0:T(1024)(128)(2,1)} %gain_second.1, bf16[1024,2816]{1,0:T(8,128)(2,1)} %gate_first.1, bf16[1024,2816]{1,0:T(8,128)(2,1)} %up_first.1, bf16[2816,1024]{1,0:T(8,128)(2,1)} %down_first.1, ...), custom_call_target="tpu_custom_call" | custom-call | tf_op jit(solution)/shard_map/pallas_call | solution.py:698
  123.7 0.8 copy.11

commit v4 on v3

--- a/solution.py
+++ b/solution.py
@@ -636,14 +636,23 @@
 
             return lax.cond(what == kind, run, lambda: counts[kind])
 
-        after = []
-        for kinds in (range(2), range(2, 4), range(4, 6), range(6, len(bodies))):
-            after += lax.cond(
-                (what >= kinds[0]) & (what <= kinds[-1]),
-                lambda: tuple(one(kind) for kind in kinds),
-                lambda: tuple(counts[kind] for kind in kinds),
+        def some(*parts):
+            kinds = [kind for part in parts for kind in part]
+
+            def run():
+                if len(parts) == 1:
+                    return tuple(one(kind) for kind in kinds)
+                return sum((some(part) for part in parts), ())
+
+            return tuple(
+                lax.cond(
+                    (what >= kinds[0]) & (what <= kinds[-1]),
+                    run,
+                    lambda: tuple(counts[kind] for kind in kinds),
+                )
             )
-        return tuple(after)
+
+        return some(range(2), range(2, 4)) + some(range(4, 6), range(6, 8), range(8, len(bodies)))
 
     done = [min(FIRST, pieces) if body is project_one else 0 for body in bodies]
     lax.fori_loop(0, length, step, tuple(jnp.int32(n) for n in done))

time: 125 us -> 123 us (0.984)
  Pallas kernels: 124 us -> 122 us
    pallas_call x1, Pallas kernels: 124 us -> 122 us  [per_device(): pl.pallas_call(functools.partial(kernel, (R, C, blocks, pieces, width, ro...]
where the time goes in v4:
time: 123 us; the launch traced here: 122 us
  Pallas kernels  122 us (99%)
    pallas_call x1, Pallas kernels, per_device(): pl.pallas_call(functools.partial(kernel, (R, C, blocks, pieces, width, ro...  122 us

profile of v4, /device:TPU:0, one launch (start us, length us, event | category | flops | bytes accessed | tf_op | source)
XLA Modules:
  0.0 122.4 jit_solution(5909620589124137241)
XLA Ops:
  0.0 121.6 %shard_map.91 = bf16[4,2,32,1024]{3,2,1,0:T(8,128)(2,1)S(1)} custom-call(bf16[4,2,32,1024]{3,2,1,0:T(8,128)(2,1)} %bitcast.3, bf16[1024]{0:T(1024)(128)(2,1)} %gain_first.1, bf16[1024]{0:T(1024)(128)(2,1)} %gain_second.1, bf16[1024,2816]{1,0:T(8,128)(2,1)} %gate_first.1, bf16[1024,2816]{1,0:T(8,128)(2,1)} %up_first.1, bf16[2816,1024]{1,0:T(8,128)(2,1)} %down_first.1, ...), custom_call_target="tpu_custom_call" | custom-call | tf_op jit(solution)/shard_map/pallas_call | solution.py:707
  121.6 0.8 copy.11
